TPU v7x, 32 devices: a whole 2x2x4 slice. The times are simulated.
32 devices in a mesh: grp: 2 (over y), ep: 8 (over z, x), tp: 2 (over core).
Axes of the slice: x: 2, y: 2, z: 4, core: 2. Of those that a mesh axis runs over, the one named last changes fastest.
Arguments:
- fresh_inputs: bfloat16 [256, 2048], P(('grp', 'ep')), parts along dimension 0, may hold values from -6 to 6
- memory_arrays: float32 [256, 32, 64, 64], P(('grp', 'ep'), 'tp'), parts along dimension 0, may hold values from -4 to 4
- chosen_specialist: int32 [256, 2], P(('grp', 'ep')), parts along dimension 0, may hold values from 0 to 3, all different within a row; in each aligned block of 128 rows (0 to 127, 128 to 255, ...) at most 96 rows name the same one
- chosen_coefficient: bfloat16 [256, 2], P(('grp', 'ep')), parts along dimension 0, may hold values from 0.25 to 1
- first_rescale: float32 [2048], replicated, may hold values from 0.1 to 1.9
- second_rescale: float32 [2048], replicated, may hold values from 0.1 to 1.9
- receiver_projector: bfloat16 [2048, 2048], P('tp', 'ep'), may hold values from -0.125 to 0.125
- address_projector: bfloat16 [2048, 2048], P('tp', 'ep'), may hold values from -0.125 to 0.125
- content_projector: bfloat16 [2048, 2048], P('tp', 'ep'), may hold values from -0.125 to 0.125
- final_projector: bfloat16 [2048, 2048], P('tp', 'ep'), may hold values from -0.125 to 0.125
- forget_narrowing: bfloat16 [2048, 64], replicated, may hold values from -0.125 to 0.125
- forget_widening: bfloat16 [64, 2048], P(None, 'tp'), may hold values from -0.75 to 0.75
- forget_bias: float32 [2048], P('tp'), may hold values from -3 to 1
- learning_narrowing: bfloat16 [2048, 64], replicated, may hold values from -0.125 to 0.125
- learning_widening: bfloat16 [64, 2048], P(None, 'tp'), may hold values from -0.75 to 0.75
- learning_bias: float32 [2048], P('tp'), may hold values from -1.5 to 1.5
- lane_scaling: float32 [2048], P('tp'), may hold values from 0.1 to 1.9
- instant_reward: float32 [32, 64], P('tp'), may hold values from -0.5 to 0.5
- specialist_switch: bfloat16 [2048, 28672], P(None, ('ep', 'tp')), may hold values from -0.125 to 0.125
- specialist_expand: bfloat16 [2048, 28672], P(None, ('ep', 'tp')), may hold values from -0.125 to 0.125
- specialist_contract: bfloat16 [28672, 2048], P(('ep', 'tp')), may hold values from -0.0625 to 0.0625
- common_activator: bfloat16 [2048, 5632], P(None, ('ep', 'tp')), may hold values from -0.125 to 0.125
- common_expand: bfloat16 [2048, 5632], P(None, ('ep', 'tp')), may hold values from -0.125 to 0.125
- common_contract: bfloat16 [5632, 2048], P(('ep', 'tp')), may hold values from -0.078125 to 0.078125
- common_switch: bfloat16 [2048], replicated, may hold values from -0.125 to 0.125
Outputs:
- new_tokens: bfloat16 [256, 2048], P(('grp', 'ep', 'tp')), parts along dimension 0
- memory_after: float32 [256, 32, 64, 64], P(('grp', 'ep'), 'tp'), parts along dimension 0
There are 2 independent parts, one for each index of `grp`. A program takes and returns all parts, laid end to end along the dimension named above; an argument that names none is the same for every part. Nothing has to cross between parts.
Inputs may be any that keep to these rules, and one draw needn't show every extreme that they name: `chosen_specialist`: each row names 2 different experts. Over the whole batch no expert is named by more than 96 rows, and in every draw some expert is named by exactly 96 rows.
All inputs are finite; a program needn't handle non-finite values.
Results may differ from a plain program's by a relative error of at most 0.014.
Values may be sent and summed in bfloat16 or wider, within the bound.
A program may use at most 128 MiB of HBM per device.

v0:
```python
import jax
import jax.numpy as jnp
from jax import lax
from jax.sharding import PartitionSpec as P

LANE_WIDTH = 64
FF_E = 7168
RMS_EPS = 1e-06
GROUP_EPS = 0.00064
HIGHEST = lax.Precision.HIGHEST


def rms_norm(values, norm_gain):
    mean_sq = jnp.mean(values * values, axis=-1, keepdims=True)
    return values * lax.rsqrt(mean_sq + RMS_EPS) * norm_gain


def widen(rounded):
    return lax.optimization_barrier(rounded).astype(jnp.float32)


def evolve_memory(
    memory_arrays,
    receiver_lanes,
    address_lanes,
    content_lanes,
    forget_lanes,
    learning_lanes,
    lane_rescale,
    instant_reward,
):
    unit_key = address_lanes * lax.rsqrt(
        jnp.sum(address_lanes * address_lanes, axis=-1, keepdims=True) + 1.0
    )
    stepped_address = address_lanes * learning_lanes
    removal = jnp.einsum("bhvk,bhk->bhv", memory_arrays, unit_key, precision=HIGHEST)
    memory_after = (
        memory_arrays * forget_lanes[:, :, None, :]
        - removal[..., None] * (unit_key * learning_lanes)[:, :, None, :]
        + content_lanes[..., None] * stepped_address[:, :, None, :]
    )
    memory_retrieval = jnp.einsum("bhvk,bhk->bhv", memory_after, receiver_lanes, precision=HIGHEST)
    centred = memory_retrieval - jnp.mean(memory_retrieval, axis=-1, keepdims=True)
    unit_address = centred * lax.rsqrt(
        jnp.mean(centred * centred, axis=-1, keepdims=True) + GROUP_EPS
    )
    instant_extra = (
        jnp.sum(receiver_lanes * stepped_address * instant_reward, axis=-1, keepdims=True)
        * content_lanes
    )
    return (memory_after, unit_address * lane_rescale + instant_extra)


def swiglu(rows_in, gate_w, up_w):
    gate_val = jnp.dot(rows_in, gate_w, preferred_element_type=jnp.float32)
    up_val = jnp.dot(rows_in, up_w, preferred_element_type=jnp.float32)
    return (jax.nn.silu(gate_val) * up_val).astype(jnp.bfloat16)


def body(
    fresh_inputs,
    memory_arrays,
    chosen_specialist,
    chosen_coefficient,
    first_rescale,
    second_rescale,
    receiver_projector,
    address_projector,
    content_projector,
    final_projector,
    forget_narrowing,
    forget_widening,
    forget_bias,
    learning_narrowing,
    learning_widening,
    learning_bias,
    lane_scaling,
    instant_reward,
    specialist_switch,
    specialist_expand,
    specialist_contract,
    common_activator,
    common_expand,
    common_contract,
    common_switch,
):
    own_rows = fresh_inputs.shape[0]
    model_width = fresh_inputs.shape[1]
    tp_count = lax.axis_size("tp")
    tp_rank = lax.axis_index("tp")
    half_width = model_width // tp_count
    head_count = half_width // LANE_WIDTH
    residual = fresh_inputs.astype(jnp.float32)
    normed = rms_norm(residual, first_rescale).astype(jnp.bfloat16)
    normed_half = lax.dynamic_slice_in_dim(normed, tp_rank * half_width, half_width, 1)
    local_weights = jnp.stack((receiver_projector, address_projector, content_projector), axis=1)
    projected_rows = jnp.einsum(
        "rd,dkc->rkc",
        lax.all_gather(normed_half, "ep", axis=0, tiled=True),
        local_weights,
        preferred_element_type=jnp.float32,
    ).astype(jnp.bfloat16)
    partial_value = lax.all_to_all(projected_rows, "ep", split_axis=0, concat_axis=2, tiled=True)
    projected = lax.psum(widen(partial_value).astype(jnp.bfloat16), "tp")
    mine = lax.dynamic_slice_in_dim(projected, tp_rank * half_width, half_width, 2)

    def divide_lanes(channels):
        return channels.astype(jnp.float32).reshape(own_rows, head_count, LANE_WIDTH)

    decay_mid = jnp.tanh(
        jnp.dot(normed, forget_narrowing, preferred_element_type=jnp.float32)
    ).astype(jnp.bfloat16)
    decay_pre = forget_bias + jnp.dot(
        decay_mid, forget_widening, preferred_element_type=jnp.float32
    )
    decay_vals = jnp.exp(-jnp.exp(-jax.nn.softplus(-decay_pre) - 0.5))
    rate_mid = jnp.dot(normed, learning_narrowing, preferred_element_type=jnp.float32).astype(
        jnp.bfloat16
    )
    rate_vals = jax.nn.sigmoid(
        learning_bias + jnp.dot(rate_mid, learning_widening, preferred_element_type=jnp.float32)
    )
    memory_after, memory_retrieval = evolve_memory(
        memory_arrays,
        divide_lanes(mine[:, 0]),
        divide_lanes(mine[:, 1]),
        divide_lanes(mine[:, 2]),
        divide_lanes(decay_vals),
        divide_lanes(rate_vals),
        lane_scaling.reshape(head_count, LANE_WIDTH),
        instant_reward,
    )
    attended = memory_retrieval.reshape(own_rows, half_width).astype(jnp.bfloat16)
    done_rows = jnp.dot(
        lax.all_gather(attended, "ep", axis=0, tiled=True),
        final_projector,
        preferred_element_type=jnp.float32,
    ).astype(jnp.bfloat16)
    out_part = lax.all_to_all(done_rows, "ep", split_axis=0, concat_axis=1, tiled=True)
    mixed_out = lax.psum(widen(out_part).astype(jnp.bfloat16), "tp")
    residual = residual + mixed_out.astype(jnp.float32)
    ffn_in = rms_norm(residual, second_rescale).astype(jnp.bfloat16)
    all_in, all_weight, all_ids = (
        lax.all_gather(ffn_in, "ep", axis=0, tiled=True),
        lax.all_gather(chosen_coefficient, "ep", axis=0, tiled=True),
        lax.all_gather(chosen_specialist, "ep", axis=0, tiled=True),
    )
    column_count = specialist_switch.shape[1]
    flat_rank = lax.axis_index("ep") * tp_count + tp_rank
    expert = flat_rank * column_count // FF_E
    expert_share = jnp.sum(
        jnp.where(all_ids == expert, all_weight.astype(jnp.float32), 0.0), axis=1
    )
    hidden = swiglu(all_in, specialist_switch, specialist_expand)
    shared_hidden = swiglu(all_in, common_activator, common_expand)
    branch_scale = jax.nn.sigmoid(
        jnp.dot(all_in, common_switch, preferred_element_type=jnp.float32)
    )
    rows_mine = own_rows // tp_count
    expert_term = expert_share[:, None] * jnp.dot(
        hidden, specialist_contract, preferred_element_type=jnp.float32
    )
    routed = lax.psum_scatter(
        expert_term
        + branch_scale[:, None]
        * jnp.dot(shared_hidden, common_contract, preferred_element_type=jnp.float32),
        ("ep", "tp"),
        scatter_dimension=0,
        tiled=True,
    )
    own_residual = lax.dynamic_slice_in_dim(residual, tp_rank * rows_mine, rows_mine, 0)
    return ((own_residual + routed).astype(jnp.bfloat16), memory_after)


def solution(mesh):
    placed = (
        P(("grp", "ep"), None),
        P(("grp", "ep"), "tp", None, None),
        P(("grp", "ep"), None),
        P(("grp", "ep"), None),
        P(),
        P(),
        P("tp", "ep"),
        P("tp", "ep"),
        P("tp", "ep"),
        P("tp", "ep"),
        P(),
        P(None, "tp"),
        P("tp"),
        P(),
        P(None, "tp"),
        P("tp"),
        P("tp"),
        P("tp", None),
        P(None, ("ep", "tp")),
        P(None, ("ep", "tp")),
        P(("ep", "tp"), None),
        P(None, ("ep", "tp")),
        P(None, ("ep", "tp")),
        P(("ep", "tp"), None),
        P(),
    )
    return jax.shard_map(
        body,
        mesh=mesh,
        in_specs=placed,
        out_specs=(P(("grp", "ep", "tp"), None), P(("grp", "ep"), "tp", None, None)),
        check_vma=False,
    )
```

profile of v0, /device:TPU:0, one launch (start us, length us, event | category | flops | bytes accessed | tf_op | source)
XLA Modules:
  0.0 324.2 jit_solution(6716720031161532944)
XLA Ops:
  7.2 0.0 copy-start
  7.2 0.0 copy-start.6
  7.2 0.0 copy-start.7
  7.2 0.0 copy-start.10
  7.2 0.0 copy-start.11
  7.2 1.1 fusion.33
  8.3 0.9 fusion.35
  9.3 32.6 %all_gather.15 = bf16[128,1024]{1,0:T(8,128)(2,1)S(1)} all-gather(bf16[16,1024]{1,0:T(8,128)(2,1)S(1)} %constant_dynamic-slice_fusion.1), channel_id=1, replica_groups=mesh['grp'=2,'ep'=8,'tp'=2] {'ep'}, dimensions={0}, use_global_device_ids=true | all-gather | bytes 294912 | tf_op jit(solution)/shard_map/all_gather | solution.py:99
  41.8 1.7 fusion.9
  43.6 0.9 copy.30
  44.5 5.5 %all-to-all-start = ((bf16[128,3,256]{2,1,0:T(4,128)(2,1)}), bf16[128,3,256]{2,1,0:T(4,128)(2,1)S(1)}, u32[]{:S(2)}, u32[]{:S(2)}) async-start(bf16[128,3,256]{2,1,0:T(4,128)(2,1)} %copy.30), calls=%async_computation | async-start | bytes 524288 | tf_op jit(solution)/shard_map/all_to_all | solution.py:103
  50.0 0.0 all-reduce.3.cloned.1.call-start
  50.0 1.4 fusion.19
  51.4 0.1 reshape.102
  51.5 6.7 %all-to-all-done = bf16[128,3,256]{2,1,0:T(4,128)(2,1)S(1)} async-done(((bf16[128,3,256]{2,1,0:T(4,128)(2,1)}), bf16[128,3,256]{2,1,0:T(4,128)(2,1)S(1)}, u32[]{:S(2)}, u32[]{:S(2)}) %all-to-all-start) | async-done | bytes 196640 | tf_op jit(solution)/shard_map/all_to_all | solution.py:103
  58.2 0.1 copy.39
  58.3 0.8 all_to_all.30
  59.1 0.0 all-reduce.3.cloned.1.call-update
  59.2 0.4 fusion.42
  59.6 0.1 mul.207
  59.7 0.1 mul.225
  59.7 15.9 %all-reduce.3.cloned.1.call-done = bf16[16,3,2048]{2,0,1:T(8,128)(2,1)} async-done(((bf16[16,3,2048]{2,0,1:T(8,128)(2,1)}), bf16[16,3,2048]{2,0,1:T(8,128)(2,1)}) %all-reduce.3.cloned.1.call-update) | async-done | bytes 196624 | tf_op jit(solution)/shard_map/psum | solution.py:104
  75.7 0.8 constant_dynamic-slice_fusion
  76.5 0.1 reshape.124
  76.6 0.1 reshape.103
  76.7 0.1 reshape.104
  76.8 0.1 multiply_reduce_fusion.2
  76.9 0.1 reshape.105
  77.0 0.1 fusion.48
  77.1 15.4 %fusion.49 = f32[16,16,1,64]{3,2,1,0:T(1,128)S(1)} fusion(f32[16,16,64,1]{2,3,1,0:T(1,128)S(1)} %bitcast.75, f32[16,16,64,64]{3,2,1,0:T(8,128)} %param.26), kind=kOutput, calls=%fused_computation.80 | convolution fusion | flops 12582912 | bytes 4325376 | tf_op jit(solution)/shard_map/bhvk,bhk->bhv/dot_general | solution.py:36
  92.5 8.6 %multiply_add_fusion = f32[16,16,64,64]{3,2,1,0:T(8,128)S(1)} fusion(f32[16,16,64,64]{3,2,1,0:T(8,128)} %param.26, f32[16,16,64]{2,1,0:T(8,128)S(1)} %get-tuple-element.4, f32[16,16,64]{2,1,0:T(8,128)S(1)} %reshape.105, f32[16,16,64]{2,1,0:T(8,128)S(1)} %get-tuple-element.2, f32[16,16,64]{2,1,0:T(8,128)S(1)} %bitcast.74, f32[16,16,64]{2,1,0:T(8,128)S(1)} %mul.207), kind=kLoop, calls=%fused_computation.1 | loop fusion | flops 5242880 | bytes 8716288 | tf_op jit(solution)/shard_map/add | solution.py:38
  101.1 0.0 copy-start.1
  101.1 3.4 %copy-done.1 = f32[16,16,64,64]{3,2,1,0:T(8,128)} copy-done((f32[16,16,64,64]{3,2,1,0:T(8,128)}, f32[16,16,64,64]{3,2,1,0:T(8,128)S(1)}, u32[]{:S(2)}) %copy-start.1) | copy-done | bytes 4194328
  104.5 0.0 copy-start.12
  104.5 0.0 copy-start.4
  104.5 0.0 copy-start.9
  104.6 6.6 %fusion.50 = f32[16,16,1,64]{3,2,1,0:T(1,128)S(1)} fusion(f32[16,16,64,64]{3,2,1,0:T(8,128)S(1)} %multiply_add_fusion, bf16[16,16,64,1]{2,3,1,0:T(2,128)(2,1)S(1)} %reshape.124), kind=kOutput, calls=%fused_computation.81 | convolution fusion | flops 12582912 | bytes 4292608 | tf_op jit(solution)/shard_map/bhvk,bhk->bhv/dot_general | solution.py:42
  111.2 0.1 reduce_sum.65
  111.3 0.2 multiply_reduce_fusion.1
  111.5 0.5 fusion.15
  112.0 0.1 convert_element_type.98
  112.2 31.1 %all_gather.16 = bf16[128,1024]{1,0:T(8,128)(2,1)S(1)} all-gather(bf16[16,1024]{1,0:T(8,128)(2,1)S(1)} %convert_element_type.98), channel_id=1, replica_groups=mesh['grp'=2,'ep'=8,'tp'=2] {'ep'}, dimensions={0}, use_global_device_ids=true | all-gather | bytes 294912 | tf_op jit(solution)/shard_map/all_gather | solution.py:135
  143.3 0.8 convolution_convert_fusion
  144.1 5.4 %all-to-all-start.1 = ((bf16[8,16,256]{2,1,0:T(8,128)(2,1)}), bf16[8,16,256]{2,1,0:T(8,128)(2,1)S(1)}, u32[]{:S(2)}, u32[]{:S(2)}) async-start(bf16[8,16,256]{2,1,0:T(8,128)(2,1)} %bitcast.12), calls=%async_computation.1 | async-start | bytes 131072 | tf_op jit(solution)/shard_map/all_to_all | solution.py:139
  149.6 0.0 all-reduce.5.cloned.1.call-start
  149.6 20.9 %all-gather.1 = bf16[8,16,2]{1,2,0:T(2,128)(2,1)S(1)} all-gather(bf16[1,16,2]{1,2,0:T(2,128)(2,1)S(1)} %bitcast.79), channel_id=1, replica_groups=mesh['grp'=2,'ep'=8,'tp'=2] {'ep'}, dimensions={0}, use_global_device_ids=true | all-gather | bytes 576 | tf_op jit(solution)/shard_map/all_gather | solution.py:145
  170.6 16.5 %all-gather = s32[8,16,2]{1,2,0:T(2,128)S(1)} all-gather(s32[1,16,2]{1,2,0:T(2,128)S(1)} %bitcast.78), channel_id=1, replica_groups=mesh['grp'=2,'ep'=8,'tp'=2] {'ep'}, dimensions={0}, use_global_device_ids=true | all-gather | bytes 1152 | tf_op jit(solution)/shard_map/all_gather | solution.py:146
  187.0 0.0 all-to-all-done.1
  187.0 0.6 copy.37
  187.6 0.0 all-reduce.5.cloned.1.call-update
  187.7 0.0 reduce-scatter.2.cloned.1.call-start
  187.7 0.1 reshape.115
  187.8 16.4 %all-reduce.5.cloned.1.call-done = bf16[16,2048]{1,0:T(8,128)(2,1)} async-done(((bf16[16,2048]{1,0:T(8,128)(2,1)}), bf16[16,2048]{1,0:T(8,128)(2,1)}) %all-reduce.5.cloned.1.call-update) | async-done | bytes 65552 | tf_op jit(solution)/shard_map/psum | solution.py:140
  204.2 1.0 convert_add_fusion
  205.2 0.9 multiply_convert_fusion
  206.1 31.8 %all_gather.19 = bf16[128,2048]{1,0:T(8,128)(2,1)S(1)} all-gather(bf16[16,2048]{1,0:T(8,128)(2,1)S(1)} %multiply_convert_fusion), channel_id=1, replica_groups=mesh['grp'=2,'ep'=8,'tp'=2] {'ep'}, dimensions={0}, use_global_device_ids=true | all-gather | bytes 589824 | tf_op jit(solution)/shard_map/all_gather | solution.py:144
  237.9 5.3 %fusion.51 = f32[128,1792]{1,0:T(8,128)} fusion(bf16[128,2048]{1,0:T(8,128)(2,1)S(1)} %all_gather.19, bf16[2048,1792]{1,0:T(8,128)(2,1)} %param.43), kind=kOutput, calls=%fused_computation.82 | convolution fusion | flops 939524096 | bytes 8781824 | tf_op jit(solution)/shard_map/dot_general | solution.py:55
  243.2 1.2 fusion.52
  244.4 0.2 fusion.25
  244.7 9.1 %convolution_multiply_fusion.1 = f32[128,2048]{1,0:T(8,128)} fusion(bf16[1792,2048]{1,0:T(8,128)(2,1)} %param.45, bf16[128,2048]{1,0:T(8,128)(2,1)S(1)} %all_gather.19, bf16[2048,1792]{1,0:T(8,128)(2,1)} %param.44, f32[128,1792]{1,0:T(8,128)} %fusion.51, f32[128]{0:T(128)S(1)} %reshape.115), kind=kOutput, calls=%fused_computation.3 | convolution fusion | flops 1880686592 | bytes 17170944 | tf_op jit(solution)/shard_map/dot_general | solution.py:160
  253.7 3.8 %fusion.1 = f32[128,2048]{1,0:T(8,128)} fusion(f32[128,2048]{1,0:T(8,128)} %convolution_multiply_fusion.1, bf16[352,2048]{1,0:T(8,128)(2,1)S(1)} %copy-done, bf16[128,2048]{1,0:T(8,128)(2,1)S(1)} %all_gather.19, bf16[2048,352]{0,1:T(8,128)(2,1)S(1)} %copy-done.3, f32[128]{0:T(128)S(1)} %fusion.25, f32[128,352]{0,1:T(8,128)} %fusion.52), kind=kOutput, calls=%fused_computation.5 | convolution fusion | flops 369893376 | bytes 5685760 | tf_op jit(solution)/shard_map/dot_general | solution.py:166
  257.5 0.0 reduce-scatter.2.cloned.1.call-update
  257.6 58.6 %reduce-scatter.2.cloned.1.call-done = f32[8,2048]{1,0:T(8,128)} async-done(((f32[128,2048]{1,0:T(8,128)}), f32[8,2048]{1,0:T(8,128)}) %reduce-scatter.2.cloned.1.call-update) | async-done | bytes 65552 | tf_op jit(solution)/shard_map/reduce_scatter | solution.py:163
  316.2 1.5 add_convert_fusion
  (28 shorter events, 0.1 us)
Async XLA Ops:
  7.2 246.6 %copy-start = (bf16[352,2048]{1,0:T(8,128)(2,1)S(1)}, bf16[352,2048]{1,0:T(8,128)(2,1)}, u32[]{:S(2)}) copy-start(bf16[352,2048]{1,0:T(8,128)(2,1)} %param.48) | copy-start | bytes 4325380
  7.2 52.0 %copy-start.6 = (bf16[2048,64]{0,1:T(8,128)(2,1)S(1)}, bf16[2048,64]{0,1:T(8,128)(2,1)}, u32[]{:S(2)}) copy-start(bf16[2048,64]{0,1:T(8,128)(2,1)} %param.35) | copy-start | bytes 786436
  7.2 52.0 %copy-start.7 = (bf16[64,1024]{1,0:T(8,128)(2,1)S(1)}, bf16[64,1024]{1,0:T(8,128)(2,1)}, u32[]{:S(2)}) copy-start(bf16[64,1024]{1,0:T(8,128)(2,1)} %param.36) | copy-start | bytes 393220
  7.2 52.0 %copy-start.10 = (f32[1024]{0:T(1024)S(1)}, f32[1024]{0:T(1024)}, u32[]{:S(2)}) copy-start(f32[1024]{0:T(1024)} %param.37) | copy-start | bytes 12292
  7.2 52.5 %copy-start.11 = (f32[1024]{0:T(1024)S(1)}, f32[1024]{0:T(1024)}, u32[]{:S(2)}) copy-start(f32[1024]{0:T(1024)} %param.41) | copy-start | bytes 12292
  44.5 13.7 %all-to-all-start = ((bf16[128,3,256]{2,1,0:T(4,128)(2,1)}), bf16[128,3,256]{2,1,0:T(4,128)(2,1)S(1)}, u32[]{:S(2)}, u32[]{:S(2)}) async-start(bf16[128,3,256]{2,1,0:T(4,128)(2,1)} %copy.30), calls=%async_computation | async-start | bytes 524288 | tf_op jit(solution)/shard_map/all_to_all | solution.py:103
  50.0 25.7 %all-reduce.3.cloned.1.call-start = ((), (), s32[]{:S(2)}) async-start(), calls=%async_computation.3 | async-start | bytes 393216 | tf_op jit(solution)/shard_map/psum | solution.py:104
  101.1 3.4 %copy-start.1 = (f32[16,16,64,64]{3,2,1,0:T(8,128)}, f32[16,16,64,64]{3,2,1,0:T(8,128)S(1)}, u32[]{:S(2)}) copy-start(f32[16,16,64,64]{3,2,1,0:T(8,128)S(1)} %multiply_add_fusion) | copy-start | bytes 12582916
  104.5 7.0 %copy-start.8 = (f32[16,64]{1,0:T(8,128)S(1)}, f32[16,64]{1,0:T(8,128)}, u32[]{:S(2)}) copy-start(f32[16,64]{1,0:T(8,128)} %param.42) | copy-start | bytes 12292
  104.5 38.8 %copy-start.5 = (bf16[1024,256]{1,0:T(8,128)(2,1)S(1)}, bf16[1024,256]{1,0:T(8,128)(2,1)}, u32[]{:S(2)}) copy-start(bf16[1024,256]{1,0:T(8,128)(2,1)} %param.34) | copy-start | bytes 1572868
  104.5 45.1 %copy-start.14 = (bf16[16,2]{0,1:T(2,128)(2,1)S(1)}, bf16[16,2]{0,1:T(2,128)(2,1)}, u32[]{:S(2)}) copy-start(bf16[16,2]{0,1:T(2,128)(2,1)} %param.28) | copy-start | bytes 196
  104.5 66.0 %copy-start.13 = (s32[16,2]{0,1:T(2,128)S(1)}, s32[16,2]{0,1:T(2,128)}, u32[]{:S(2)}) copy-start(s32[16,2]{0,1:T(2,128)} %param.27) | copy-start | bytes 388
  104.5 83.3 %copy-start.12 = (bf16[2048]{0:T(1024)(128)(2,1)S(1)}, bf16[2048]{0:T(1024)(128)(2,1)}, u32[]{:S(2)}) copy-start(bf16[2048]{0:T(1024)(128)(2,1)} %param.49) | copy-start | bytes 12292
  104.5 99.7 %copy-start.4 = (bf16[16,2048]{1,0:T(8,128)(2,1)S(1)}, bf16[16,2048]{1,0:T(8,128)(2,1)}, u32[]{:S(2)}) copy-start(bf16[16,2048]{1,0:T(8,128)(2,1)} %param.25) | copy-start | bytes 196612
  104.5 100.7 %copy-start.9 = (f32[2048]{0:T(1024)S(1)}, f32[2048]{0:T(1024)}, u32[]{:S(2)}) copy-start(f32[2048]{0:T(1024)} %param.30) | copy-start | bytes 24580
  144.1 42.9 %all-to-all-start.1 = ((bf16[8,16,256]{2,1,0:T(8,128)(2,1)}), bf16[8,16,256]{2,1,0:T(8,128)(2,1)S(1)}, u32[]{:S(2)}, u32[]{:S(2)}) async-start(bf16[8,16,256]{2,1,0:T(8,128)(2,1)} %bitcast.12), calls=%async_computation.1 | async-start | bytes 131072 | tf_op jit(solution)/shard_map/all_to_all | solution.py:139
  149.6 54.7 %all-reduce.5.cloned.1.call-start = ((), (), s32[]{:S(2)}) async-start(), calls=%async_computation.4 | async-start | bytes 131072 | tf_op jit(solution)/shard_map/psum | solution.py:140
  187.7 128.5 %reduce-scatter.2.cloned.1.call-start = ((), (), s32[]{:S(2)}) async-start(), calls=%async_computation.5 | async-start | bytes 1114112 | tf_op jit(solution)/shard_map/reduce_scatter | solution.py:163
  237.9 5.3 %copy-start.2 = (bf16[2048,352]{0,1:T(8,128)(2,1)S(1)}, bf16[2048,352]{0,1:T(8,128)(2,1)}, u32[]{:S(2)}) copy-start(bf16[2048,352]{0,1:T(8,128)(2,1)} %param.46) | copy-start | bytes 4325380
  244.7 9.1 %copy-start.3 = (bf16[2048,352]{0,1:T(8,128)(2,1)S(1)}, bf16[2048,352]{0,1:T(8,128)(2,1)}, u32[]{:S(2)}) copy-start(bf16[2048,352]{0,1:T(8,128)(2,1)} %param.47) | copy-start | bytes 4325380
Sparse Core Ops, SparseCore 0:
  59.3 16.3 all-reduce.2
  187.8 16.3 all-reduce.4
  257.7 58.4 reduce-scatter.1
where the time goes:
time: 325 us; the launch traced here: 324 us
  blocking collectives  133 us (41%)
  waiting for transfers between devices  97.7 us (30%)
  matrix products  46 us (14%)
  other arithmetic  15.8 us (5%)
  between operations  14.1 us (4%)
  starting transfers between devices  11.1 us (3%)
  local copies, waits for them, and re-layouts  6.74 us (2%)
    reduce_scatter x1, waiting for transfers between devices, body(): lax.psum_scatter(expert_term + branch_scale[:, None] * jnp.dot(shared_hid...  58.6 us
    all_gather x1, blocking collectives, body(): lax.all_gather(normed_half, 'ep', axis=0, tiled=True)  32.6 us
    all_gather x1, blocking collectives, body(): lax.all_gather(ffn_in, 'ep', axis=0, tiled=True)  31.8 us
    all_gather x1, blocking collectives, body(): lax.all_gather(attended, 'ep', axis=0, tiled=True)  31.1 us
    all_gather x1, blocking collectives, body(): lax.all_gather(chosen_coefficient, 'ep', axis=0, tiled=True)  20.9 us
    all_gather x1, blocking collectives, body(): lax.all_gather(chosen_specialist, 'ep', axis=0, tiled=True)  16.5 us
    psum x1, waiting for transfers between devices, body(): mixed_out = lax.psum(widen(out_part).astype(jnp.bfloat16), 'tp')  16.4 us
    psum x1, waiting for transfers between devices, body(): projected = lax.psum(widen(partial_value).astype(jnp.bfloat16), 'tp')  15.9 us
  transfers between devices with their start and end apart: 5, of which 4 were waited for; matrix products, arithmetic and copies ran while one was open for 1% of the time, Pallas kernels for 0%

commit v1 on v0

--- a/solution.py
+++ b/solution.py
@@ -8,6 +8,20 @@
 RMS_EPS = 1e-06
 GROUP_EPS = 0.00064
 HIGHEST = lax.Precision.HIGHEST
+
+
+def work_both_ways(shard, axis, dim, make, out_dim):
+    ways, here, step = (lax.axis_size(axis), lax.axis_index(axis), shard.shape[dim])
+    earlier, later = ([], [])
+    going_up = going_down = shard
+    for far in range(ways // 2 + 1):
+        earlier.append(make(going_up, (here - far) % ways * step))
+        if 0 < far < ways - ways // 2:
+            later.append(make(going_down, (here + far) % ways * step))
+        going_up = lax.ppermute(going_up, axis, [(d, (d + 1) % ways) for d in range(ways)])
+        going_down = lax.ppermute(going_down, axis, [(d, (d - 1) % ways) for d in range(ways)])
+    line = jnp.concatenate([*earlier[::-1], *later], axis=out_dim)
+    return jnp.roll(line, (here - ways // 2) * earlier[0].shape[out_dim], axis=out_dim)
 
 
 def rms_norm(values, norm_gain):
@@ -94,11 +108,14 @@
     normed = rms_norm(residual, first_rescale).astype(jnp.bfloat16)
     normed_half = lax.dynamic_slice_in_dim(normed, tp_rank * half_width, half_width, 1)
     local_weights = jnp.stack((receiver_projector, address_projector, content_projector), axis=1)
-    projected_rows = jnp.einsum(
-        "rd,dkc->rkc",
-        lax.all_gather(normed_half, "ep", axis=0, tiled=True),
-        local_weights,
-        preferred_element_type=jnp.float32,
+    projected_rows = work_both_ways(
+        normed_half,
+        "ep",
+        0,
+        lambda part, offset: jnp.einsum(
+            "rd,dkc->rkc", part, local_weights, preferred_element_type=jnp.float32
+        ),
+        0,
     ).astype(jnp.bfloat16)
     partial_value = lax.all_to_all(projected_rows, "ep", split_axis=0, concat_axis=2, tiled=True)
     projected = lax.psum(widen(partial_value).astype(jnp.bfloat16), "tp")

time: 325 us -> 318 us (0.978)
  blocking collectives: 133 us -> 100 us
  starting transfers between devices: 11.1 us -> 26.2 us
  waiting for transfers between devices: 97.7 us -> 109 us
  local copies, waits for them, and re-layouts: 6.74 us -> 3.47 us
    all_gather x1 -> x0, blocking collectives: 32.6 us -> none  [body(): lax.all_gather(normed_half, 'ep', axis=0, tiled=True)]
    ppermute x0 -> x7, starting transfers between devices: none -> 17.2 us  [the longest x3 14.2 us: work_both_ways(): lax.ppermute(going_down, axis, [(d, (d - 1) % ways) for d in range(ways)])]
    ppermute x0 -> x7, waiting for transfers between devices: none -> 10.6 us  [the longest x4 10.6 us: work_both_ways(): lax.ppermute(going_up, axis, [(d, (d + 1) % ways) for d in range(ways)])]
    unnamed x31 -> x52, local copies, waits for them, and re-layouts: 3.47 us -> 0.17 us
  transfers between devices with their start and end apart: 5 -> 12, of which waited for: 4 -> 8; matrix products, arithmetic and copies ran while one was open for 1% -> 2% of each run, Pallas kernels for 0% -> 0%
where the time goes in v1:
time: 318 us; the launch traced here: 317 us
  waiting for transfers between devices  109 us (34%)
  blocking collectives  100 us (31%)
  matrix products  47.4 us (15%)
  starting transfers between devices  26.2 us (8%)
  other arithmetic  15.8 us (5%)
  between operations  14.2 us (4%)
  local copies, waits for them, and re-layouts  3.47 us (1%)
    reduce_scatter x1, waiting for transfers between devices, body(): lax.psum_scatter(expert_term + branch_scale[:, None] * jnp.dot(shared_hid...  58.6 us
    all_gather x1, blocking collectives, body(): lax.all_gather(ffn_in, 'ep', axis=0, tiled=True)  31.8 us
    all_gather x1, blocking collectives, body(): lax.all_gather(attended, 'ep', axis=0, tiled=True)  31.1 us
    all_gather x1, blocking collectives, body(): lax.all_gather(chosen_coefficient, 'ep', axis=0, tiled=True)  20.9 us
    all_gather x1, blocking collectives, body(): lax.all_gather(chosen_specialist, 'ep', axis=0, tiled=True)  16.5 us
    psum x1, waiting for transfers between devices, body(): mixed_out = lax.psum(widen(out_part).astype(jnp.bfloat16), 'tp')  16.4 us
    psum x1, waiting for transfers between devices, body(): projected = lax.psum(widen(partial_value).astype(jnp.bfloat16), 'tp')  16.1 us
    dot_general x1, matrix products, evolve_memory(): jnp.einsum('bhvk,bhk->bhv', memory_arrays, unit_key, precision=HIGHEST)  15.6 us
  transfers between devices with their start and end apart: 12, of which 8 were waited for; matrix products, arithmetic and copies ran while one was open for 2% of the time, Pallas kernels for 0%

profile of v1, /device:TPU:0, one launch (start us, length us, event | category | flops | bytes accessed | tf_op | source)
XLA Modules:
  0.0 316.7 jit_solution(11669022693761636242)
XLA Ops:
  7.2 1.1 fusion.23
  8.3 0.9 fusion.25
  9.3 3.0 collective-permute-start
  12.3 4.9 %collective-permute-done = bf16[16,1024]{1,0:T(8,128)(2,1)S(1)} collective-permute-done((bf16[16,1024]{1,0:T(8,128)(2,1)S(1)}, bf16[16,1024]{1,0:T(8,128)(2,1)S(1)}, u32[]{:S(2)}, u32[]{:S(2)}) %collective-permute-start) | collective-permute-done | bytes 32800 | tf_op jit(solution)/shard_map/ppermute | solution.py:21
  17.2 4.7 %collective-permute-start.4 = (bf16[16,1024]{1,0:T(8,128)(2,1)S(1)}, bf16[16,1024]{1,0:T(8,128)(2,1)S(1)}, u32[]{:S(2)}, u32[]{:S(2)}) collective-permute-start(bf16[16,1024]{1,0:T(8,128)(2,1)S(1)} %constant_dynamic-slice_fusion.1), channel_id=1, source_target_pairs={{0,14},{2,0},{4,2},{6,4},{8,6},{10,8},{12,10},{14,12},{1,15},{3,1}... | collective-permute-start | bytes 98312 | tf_op jit(solution)/shard_map/ppermute | solution.py:22
  22.0 1.9 collective-permute-done.1
  23.9 4.7 %collective-permute-start.5 = (bf16[16,1024]{1,0:T(8,128)(2,1)S(1)}, bf16[16,1024]{1,0:T(8,128)(2,1)S(1)}, u32[]{:S(2)}, u32[]{:S(2)}) collective-permute-start(bf16[16,1024]{1,0:T(8,128)(2,1)S(1)} %collective-permute-done.4), channel_id=1, source_target_pairs={{0,14},{2,0},{4,2},{6,4},{8,6},{10,8},{12,10},{14,12},{1,15},{3,1}... | collective-permute-start | bytes 98312 | tf_op jit(solution)/shard_map/ppermute | solution.py:22
  28.6 1.9 collective-permute-done.2
  30.5 4.7 %collective-permute-start.6 = (bf16[16,1024]{1,0:T(8,128)(2,1)S(1)}, bf16[16,1024]{1,0:T(8,128)(2,1)S(1)}, u32[]{:S(2)}, u32[]{:S(2)}) collective-permute-start(bf16[16,1024]{1,0:T(8,128)(2,1)S(1)} %collective-permute-done.5), channel_id=1, source_target_pairs={{0,14},{2,0},{4,2},{6,4},{8,6},{10,8},{12,10},{14,12},{1,15},{3,1}... | collective-permute-start | bytes 98312 | tf_op jit(solution)/shard_map/ppermute | solution.py:22
  35.2 1.9 collective-permute-done.3
  37.1 1.7 constant_dynamic-update-slice_fusion.15
  38.9 0.3 constant_dynamic-update-slice_fusion.14
  39.2 0.3 constant_dynamic-update-slice_fusion.13
  39.5 0.3 constant_dynamic-update-slice_fusion.12
  39.8 0.3 constant_dynamic-update-slice_fusion.11
  40.2 0.3 constant_dynamic-update-slice_fusion.10
  40.5 0.3 constant_dynamic-update-slice_fusion.9
  40.9 0.3 constant_dynamic-update-slice_fusion.8
  41.3 0.9 copy.30
  42.2 3.4 %all-to-all-start = ((bf16[128,3,256]{2,1,0:T(4,128)(2,1)}), bf16[128,3,256]{2,1,0:T(4,128)(2,1)S(1)}, u32[]{:S(2)}, u32[]{:S(2)}) async-start(bf16[128,3,256]{2,1,0:T(4,128)(2,1)} %copy.30), calls=%async_computation | async-start | bytes 524288 | tf_op jit(solution)/shard_map/all_to_all | solution.py:120
  45.6 0.0 all-reduce.3.cloned.1.call-start
  45.7 0.4 fusion.10
  46.1 0.1 reshape.102
  46.2 7.6 %all-to-all-done = bf16[128,3,256]{2,1,0:T(4,128)(2,1)S(1)} async-done(((bf16[128,3,256]{2,1,0:T(4,128)(2,1)}), bf16[128,3,256]{2,1,0:T(4,128)(2,1)S(1)}, u32[]{:S(2)}, u32[]{:S(2)}) %all-to-all-start) | async-done | bytes 196640 | tf_op jit(solution)/shard_map/all_to_all | solution.py:120
  53.8 0.1 copy.39
  53.9 0.8 all_to_all.30
  54.8 0.4 fusion.32
  55.2 0.1 mul.210
  55.3 0.1 mul.229
  55.3 16.1 %all-reduce.3.cloned.1.call-done = bf16[16,3,2048]{2,0,1:T(8,128)(2,1)} async-done(((bf16[16,3,2048]{2,0,1:T(8,128)(2,1)}), bf16[16,3,2048]{2,0,1:T(8,128)(2,1)}) %all-reduce.3.cloned.1.call-update) | async-done | bytes 196624 | tf_op jit(solution)/shard_map/psum | solution.py:121
  71.4 0.8 constant_dynamic-slice_fusion
  72.2 0.1 reshape.131
  72.3 0.1 reshape.103
  72.5 0.1 reshape.104
  72.5 0.1 multiply_reduce_fusion.2
  72.7 0.1 reshape.105
  72.8 0.1 fusion.53
  72.9 15.6 %fusion.54 = f32[16,16,1,64]{3,2,1,0:T(1,128)S(1)} fusion(f32[16,16,64,1]{2,3,1,0:T(1,128)S(1)} %bitcast.112, f32[16,16,64,64]{3,2,1,0:T(8,128)} %param.26), kind=kOutput, calls=%fused_computation.105 | convolution fusion | flops 12582912 | bytes 4325376 | tf_op jit(solution)/shard_map/bhvk,bhk->bhv/dot_general | solution.py:50
  88.5 8.6 %multiply_add_fusion = f32[16,16,64,64]{3,2,1,0:T(8,128)S(1)} fusion(f32[16,16,64,64]{3,2,1,0:T(8,128)} %param.26, f32[16,16,64]{2,1,0:T(8,128)S(1)} %get-tuple-element.4, f32[16,16,64]{2,1,0:T(8,128)S(1)} %reshape.105, f32[16,16,64]{2,1,0:T(8,128)S(1)} %get-tuple-element.2, f32[16,16,64]{2,1,0:T(8,128)S(1)} %bitcast.111, f32[16,16,64]{2,1,0:T(8,128)S(1)} %mul.210), kind=kLoop, calls=%fused_computation.1 | loop fusion | flops 5242880 | bytes 8716288 | tf_op jit(solution)/shard_map/add | solution.py:52
  97.1 6.6 %fusion.55 = f32[16,16,1,64]{3,2,1,0:T(1,128)S(1)} fusion(f32[16,16,64,64]{3,2,1,0:T(8,128)S(1)} %multiply_add_fusion, bf16[16,16,64,1]{2,3,1,0:T(2,128)(2,1)S(1)} %reshape.131), kind=kOutput, calls=%fused_computation.106 | convolution fusion | flops 12582912 | bytes 4292608 | tf_op jit(solution)/shard_map/bhvk,bhk->bhv/dot_general | solution.py:56
  103.7 0.1 reduce_sum.65
  103.8 0.2 multiply_reduce_fusion.1
  104.1 0.5 fusion.6
  104.6 0.1 convert_element_type.98
  104.7 31.1 %all_gather.12 = bf16[128,1024]{1,0:T(8,128)(2,1)S(1)} all-gather(bf16[16,1024]{1,0:T(8,128)(2,1)S(1)} %convert_element_type.98), channel_id=1, replica_groups=mesh['grp'=2,'ep'=8,'tp'=2] {'ep'}, dimensions={0}, use_global_device_ids=true | all-gather | bytes 294912 | tf_op jit(solution)/shard_map/all_gather | solution.py:152
  135.8 0.9 convolution_convert_fusion
  136.7 5.4 %all-to-all-start.1 = ((bf16[8,16,256]{2,1,0:T(8,128)(2,1)}), bf16[8,16,256]{2,1,0:T(8,128)(2,1)S(1)}, u32[]{:S(2)}, u32[]{:S(2)}) async-start(bf16[8,16,256]{2,1,0:T(8,128)(2,1)} %bitcast.19), calls=%async_computation.1 | async-start | bytes 131072 | tf_op jit(solution)/shard_map/all_to_all | solution.py:156
  142.1 0.0 all-reduce.5.cloned.1.call-start
  142.2 20.9 %all-gather.1 = bf16[8,16,2]{1,2,0:T(2,128)(2,1)S(1)} all-gather(bf16[1,16,2]{1,2,0:T(2,128)(2,1)S(1)} %bitcast.116), channel_id=1, replica_groups=mesh['grp'=2,'ep'=8,'tp'=2] {'ep'}, dimensions={0}, use_global_device_ids=true | all-gather | bytes 576 | tf_op jit(solution)/shard_map/all_gather | solution.py:162
  163.1 16.5 %all-gather = s32[8,16,2]{1,2,0:T(2,128)S(1)} all-gather(s32[1,16,2]{1,2,0:T(2,128)S(1)} %bitcast.115), channel_id=1, replica_groups=mesh['grp'=2,'ep'=8,'tp'=2] {'ep'}, dimensions={0}, use_global_device_ids=true | all-gather | bytes 1152 | tf_op jit(solution)/shard_map/all_gather | solution.py:163
  179.6 0.6 copy.37
  180.3 0.0 reduce-scatter.2.cloned.1.call-start
  180.3 0.1 reshape.115
  180.4 16.4 %all-reduce.5.cloned.1.call-done = bf16[16,2048]{1,0:T(8,128)(2,1)} async-done(((bf16[16,2048]{1,0:T(8,128)(2,1)}), bf16[16,2048]{1,0:T(8,128)(2,1)}) %all-reduce.5.cloned.1.call-update) | async-done | bytes 65552 | tf_op jit(solution)/shard_map/psum | solution.py:157
  196.8 1.0 convert_add_fusion
  197.8 0.9 multiply_convert_fusion
  198.8 31.8 %all_gather.15 = bf16[128,2048]{1,0:T(8,128)(2,1)S(1)} all-gather(bf16[16,2048]{1,0:T(8,128)(2,1)S(1)} %multiply_convert_fusion), channel_id=1, replica_groups=mesh['grp'=2,'ep'=8,'tp'=2] {'ep'}, dimensions={0}, use_global_device_ids=true | all-gather | bytes 589824 | tf_op jit(solution)/shard_map/all_gather | solution.py:161
  230.5 5.3 %fusion.56 = f32[128,1792]{1,0:T(8,128)} fusion(bf16[128,2048]{1,0:T(8,128)(2,1)S(1)} %all_gather.15, bf16[2048,1792]{1,0:T(8,128)(2,1)} %param.43), kind=kOutput, calls=%fused_computation.107 | convolution fusion | flops 939524096 | bytes 8781824 | tf_op jit(solution)/shard_map/dot_general | solution.py:69
  235.8 1.2 fusion.57
  237.0 0.2 fusion.16
  237.2 9.1 %convolution_multiply_fusion.1 = f32[128,2048]{1,0:T(8,128)} fusion(bf16[1792,2048]{1,0:T(8,128)(2,1)} %param.45, bf16[128,2048]{1,0:T(8,128)(2,1)S(1)} %all_gather.15, bf16[2048,1792]{1,0:T(8,128)(2,1)} %param.44, f32[128,1792]{1,0:T(8,128)} %fusion.56, f32[128]{0:T(128)S(1)} %reshape.115), kind=kOutput, calls=%fused_computation.3 | convolution fusion | flops 1880686592 | bytes 17170944 | tf_op jit(solution)/shard_map/dot_general | solution.py:177
  246.3 3.8 %fusion.1 = f32[128,2048]{1,0:T(8,128)} fusion(f32[128,2048]{1,0:T(8,128)} %convolution_multiply_fusion.1, bf16[352,2048]{1,0:T(8,128)(2,1)S(1)} %copy-done, bf16[128,2048]{1,0:T(8,128)(2,1)S(1)} %all_gather.15, bf16[2048,352]{0,1:T(8,128)(2,1)S(1)} %copy-done.3, f32[128]{0:T(128)S(1)} %fusion.16, f32[128,352]{0,1:T(8,128)} %fusion.57), kind=kOutput, calls=%fused_computation.5 | convolution fusion | flops 369893376 | bytes 5685760 | tf_op jit(solution)/shard_map/dot_general | solution.py:183
  250.1 58.6 %reduce-scatter.2.cloned.1.call-done = f32[8,2048]{1,0:T(8,128)} async-done(((f32[128,2048]{1,0:T(8,128)}), f32[8,2048]{1,0:T(8,128)}) %reduce-scatter.2.cloned.1.call-update) | async-done | bytes 65552 | tf_op jit(solution)/shard_map/reduce_scatter | solution.py:180
  308.8 1.5 add_convert_fusion
  (71 shorter events, 0.3 us)
Async XLA Ops:
  7.2 239.2 %copy-start = (bf16[352,2048]{1,0:T(8,128)(2,1)S(1)}, bf16[352,2048]{1,0:T(8,128)(2,1)}, u32[]{:S(2)}) copy-start(bf16[352,2048]{1,0:T(8,128)(2,1)} %param.48) | copy-start | bytes 4325380
  7.2 31.7 %copy-start.16 = (bf16[1024,256]{1,0:T(8,128)(2,1)S(1)}, bf16[1024,256]{1,0:T(8,128)(2,1)}, u32[]{:S(2)}) copy-start(bf16[1024,256]{1,0:T(8,128)(2,1)} %param.32) | copy-start | bytes 1572868
  7.2 31.7 %copy-start.15 = (bf16[1024,256]{1,0:T(8,128)(2,1)S(1)}, bf16[1024,256]{1,0:T(8,128)(2,1)}, u32[]{:S(2)}) copy-start(bf16[1024,256]{1,0:T(8,128)(2,1)} %param.33) | copy-start | bytes 1572868
  9.3 8.0 %collective-permute-start = (bf16[16,1024]{1,0:T(8,128)(2,1)S(1)}, bf16[16,1024]{1,0:T(8,128)(2,1)S(1)}, u32[]{:S(2)}, u32[]{:S(2)}) collective-permute-start(bf16[16,1024]{1,0:T(8,128)(2,1)S(1)} %constant_dynamic-slice_fusion.1), channel_id=1, source_target_pairs={{0,2},{2,4},{4,6},{6,8},{8,10},{10,12},{12,14},{14,0},{1,3},{3,5},... | collective-permute-start | bytes 98312 | tf_op jit(solution)/shard_map/ppermute | solution.py:21
  17.2 6.6 %collective-permute-start.1 = (bf16[16,1024]{1,0:T(8,128)(2,1)S(1)}, bf16[16,1024]{1,0:T(8,128)(2,1)S(1)}, u32[]{:S(2)}, u32[]{:S(2)}) collective-permute-start(bf16[16,1024]{1,0:T(8,128)(2,1)S(1)} %collective-permute-done), channel_id=1, source_target_pairs={{0,2},{2,4},{4,6},{6,8},{8,10},{10,12},{12,14},{14,0},{1,3},{3,5},... | collective-permute-start | bytes 98312 | tf_op jit(solution)/shard_map/ppermute | solution.py:21
  17.2 6.6 %collective-permute-start.4 = (bf16[16,1024]{1,0:T(8,128)(2,1)S(1)}, bf16[16,1024]{1,0:T(8,128)(2,1)S(1)}, u32[]{:S(2)}, u32[]{:S(2)}) collective-permute-start(bf16[16,1024]{1,0:T(8,128)(2,1)S(1)} %constant_dynamic-slice_fusion.1), channel_id=1, source_target_pairs={{0,14},{2,0},{4,2},{6,4},{8,6},{10,8},{12,10},{14,12},{1,15},{3,1}... | collective-permute-start | bytes 98312 | tf_op jit(solution)/shard_map/ppermute | solution.py:22
  23.9 6.6 %collective-permute-start.2 = (bf16[16,1024]{1,0:T(8,128)(2,1)S(1)}, bf16[16,1024]{1,0:T(8,128)(2,1)S(1)}, u32[]{:S(2)}, u32[]{:S(2)}) collective-permute-start(bf16[16,1024]{1,0:T(8,128)(2,1)S(1)} %collective-permute-done.1), channel_id=1, source_target_pairs={{0,2},{2,4},{4,6},{6,8},{8,10},{10,12},{12,14},{14,0},{1,3},{3,5},... | collective-permute-start | bytes 98312 | tf_op jit(solution)/shard_map/ppermute | solution.py:21
  23.9 6.6 %collective-permute-start.5 = (bf16[16,1024]{1,0:T(8,128)(2,1)S(1)}, bf16[16,1024]{1,0:T(8,128)(2,1)S(1)}, u32[]{:S(2)}, u32[]{:S(2)}) collective-permute-start(bf16[16,1024]{1,0:T(8,128)(2,1)S(1)} %collective-permute-done.4), channel_id=1, source_target_pairs={{0,14},{2,0},{4,2},{6,4},{8,6},{10,8},{12,10},{14,12},{1,15},{3,1}... | collective-permute-start | bytes 98312 | tf_op jit(solution)/shard_map/ppermute | solution.py:22
  30.5 6.6 %collective-permute-start.3 = (bf16[16,1024]{1,0:T(8,128)(2,1)S(1)}, bf16[16,1024]{1,0:T(8,128)(2,1)S(1)}, u32[]{:S(2)}, u32[]{:S(2)}) collective-permute-start(bf16[16,1024]{1,0:T(8,128)(2,1)S(1)} %collective-permute-done.2), channel_id=1, source_target_pairs={{0,2},{2,4},{4,6},{6,8},{8,10},{10,12},{12,14},{14,0},{1,3},{3,5},... | collective-permute-start | bytes 98312 | tf_op jit(solution)/shard_map/ppermute | solution.py:21
  30.5 8.4 %copy-start.18 = (bf16[1024,256]{1,0:T(8,128)(2,1)S(1)}, bf16[1024,256]{1,0:T(8,128)(2,1)}, u32[]{:S(2)}) copy-start(bf16[1024,256]{1,0:T(8,128)(2,1)} %param.31) | copy-start | bytes 1572868
  30.5 10.3 %collective-permute-start.6 = (bf16[16,1024]{1,0:T(8,128)(2,1)S(1)}, bf16[16,1024]{1,0:T(8,128)(2,1)S(1)}, u32[]{:S(2)}, u32[]{:S(2)}) collective-permute-start(bf16[16,1024]{1,0:T(8,128)(2,1)S(1)} %collective-permute-done.5), channel_id=1, source_target_pairs={{0,14},{2,0},{4,2},{6,4},{8,6},{10,8},{12,10},{14,12},{1,15},{3,1}... | collective-permute-start | bytes 98312 | tf_op jit(solution)/shard_map/ppermute | solution.py:22
  37.1 2.1 copy-start.17
  40.8 4.9 %copy-start.19 = (bf16[2048,64]{0,1:T(8,128)(2,1)S(1)}, bf16[2048,64]{0,1:T(8,128)(2,1)}, u32[]{:S(2)}) copy-start(bf16[2048,64]{0,1:T(8,128)(2,1)} %param.38) | copy-start | bytes 786436
  40.8 4.9 %copy-start.20 = (bf16[64,1024]{1,0:T(8,128)(2,1)S(1)}, bf16[64,1024]{1,0:T(8,128)(2,1)}, u32[]{:S(2)}) copy-start(bf16[64,1024]{1,0:T(8,128)(2,1)} %param.39) | copy-start | bytes 393220
  40.8 4.9 %copy-start.21 = (f32[1024]{0:T(1024)S(1)}, f32[1024]{0:T(1024)}, u32[]{:S(2)}) copy-start(f32[1024]{0:T(1024)} %param.40) | copy-start | bytes 12292
  40.8 13.9 %copy-start.6 = (bf16[2048,64]{0,1:T(8,128)(2,1)S(1)}, bf16[2048,64]{0,1:T(8,128)(2,1)}, u32[]{:S(2)}) copy-start(bf16[2048,64]{0,1:T(8,128)(2,1)} %param.35) | copy-start | bytes 786436
  40.9 13.9 %copy-start.7 = (bf16[64,1024]{1,0:T(8,128)(2,1)S(1)}, bf16[64,1024]{1,0:T(8,128)(2,1)}, u32[]{:S(2)}) copy-start(bf16[64,1024]{1,0:T(8,128)(2,1)} %param.36) | copy-start | bytes 393220
  40.9 13.9 %copy-start.10 = (f32[1024]{0:T(1024)S(1)}, f32[1024]{0:T(1024)}, u32[]{:S(2)}) copy-start(f32[1024]{0:T(1024)} %param.37) | copy-start | bytes 12292
  40.9 14.4 %copy-start.11 = (f32[1024]{0:T(1024)S(1)}, f32[1024]{0:T(1024)}, u32[]{:S(2)}) copy-start(f32[1024]{0:T(1024)} %param.41) | copy-start | bytes 12292
  42.2 11.6 %all-to-all-start = ((bf16[128,3,256]{2,1,0:T(4,128)(2,1)}), bf16[128,3,256]{2,1,0:T(4,128)(2,1)S(1)}, u32[]{:S(2)}, u32[]{:S(2)}) async-start(bf16[128,3,256]{2,1,0:T(4,128)(2,1)} %copy.30), calls=%async_computation | async-start | bytes 524288 | tf_op jit(solution)/shard_map/all_to_all | solution.py:120
  45.6 25.8 %all-reduce.3.cloned.1.call-start = ((), (), s32[]{:S(2)}) async-start(), calls=%async_computation.3 | async-start | bytes 393216 | tf_op jit(solution)/shard_map/psum | solution.py:121
  97.0 6.7 %copy-start.1 = (f32[16,16,64,64]{3,2,1,0:T(8,128)}, f32[16,16,64,64]{3,2,1,0:T(8,128)S(1)}, u32[]{:S(2)}) copy-start(f32[16,16,64,64]{3,2,1,0:T(8,128)S(1)} %multiply_add_fusion) | copy-start | bytes 12582916
  97.0 7.0 %copy-start.8 = (f32[16,64]{1,0:T(8,128)S(1)}, f32[16,64]{1,0:T(8,128)}, u32[]{:S(2)}) copy-start(f32[16,64]{1,0:T(8,128)} %param.42) | copy-start | bytes 12292
  97.0 38.8 %copy-start.5 = (bf16[1024,256]{1,0:T(8,128)(2,1)S(1)}, bf16[1024,256]{1,0:T(8,128)(2,1)}, u32[]{:S(2)}) copy-start(bf16[1024,256]{1,0:T(8,128)(2,1)} %param.34) | copy-start | bytes 1572868
  97.0 45.2 %copy-start.14 = (bf16[16,2]{0,1:T(2,128)(2,1)S(1)}, bf16[16,2]{0,1:T(2,128)(2,1)}, u32[]{:S(2)}) copy-start(bf16[16,2]{0,1:T(2,128)(2,1)} %param.28) | copy-start | bytes 196
  97.1 66.1 %copy-start.13 = (s32[16,2]{0,1:T(2,128)S(1)}, s32[16,2]{0,1:T(2,128)}, u32[]{:S(2)}) copy-start(s32[16,2]{0,1:T(2,128)} %param.27) | copy-start | bytes 388
  97.1 83.4 %copy-start.12 = (bf16[2048]{0:T(1024)(128)(2,1)S(1)}, bf16[2048]{0:T(1024)(128)(2,1)}, u32[]{:S(2)}) copy-start(bf16[2048]{0:T(1024)(128)(2,1)} %param.49) | copy-start | bytes 12292
  97.1 99.7 %copy-start.4 = (bf16[16,2048]{1,0:T(8,128)(2,1)S(1)}, bf16[16,2048]{1,0:T(8,128)(2,1)}, u32[]{:S(2)}) copy-start(bf16[16,2048]{1,0:T(8,128)(2,1)} %param.25) | copy-start | bytes 196612
  97.1 100.7 %copy-start.9 = (f32[2048]{0:T(1024)S(1)}, f32[2048]{0:T(1024)}, u32[]{:S(2)}) copy-start(f32[2048]{0:T(1024)} %param.30) | copy-start | bytes 24580
  136.7 42.9 %all-to-all-start.1 = ((bf16[8,16,256]{2,1,0:T(8,128)(2,1)}), bf16[8,16,256]{2,1,0:T(8,128)(2,1)S(1)}, u32[]{:S(2)}, u32[]{:S(2)}) async-start(bf16[8,16,256]{2,1,0:T(8,128)(2,1)} %bitcast.19), calls=%async_computation.1 | async-start | bytes 131072 | tf_op jit(solution)/shard_map/all_to_all | solution.py:156
  142.1 54.7 %all-reduce.5.cloned.1.call-start = ((), (), s32[]{:S(2)}) async-start(), calls=%async_computation.4 | async-start | bytes 131072 | tf_op jit(solution)/shard_map/psum | solution.py:157
  180.3 128.5 %reduce-scatter.2.cloned.1.call-start = ((), (), s32[]{:S(2)}) async-start(), calls=%async_computation.5 | async-start | bytes 1114112 | tf_op jit(solution)/shard_map/reduce_scatter | solution.py:180
  230.5 5.3 %copy-start.2 = (bf16[2048,352]{0,1:T(8,128)(2,1)S(1)}, bf16[2048,352]{0,1:T(8,128)(2,1)}, u32[]{:S(2)}) copy-start(bf16[2048,352]{0,1:T(8,128)(2,1)} %param.46) | copy-start | bytes 4325380
  237.2 9.1 %copy-start.3 = (bf16[2048,352]{0,1:T(8,128)(2,1)S(1)}, bf16[2048,352]{0,1:T(8,128)(2,1)}, u32[]{:S(2)}) copy-start(bf16[2048,352]{0,1:T(8,128)(2,1)} %param.47) | copy-start | bytes 4325380
Sparse Core Ops, SparseCore 0:
  54.9 16.5 all-reduce.2
  180.4 16.3 all-reduce.4
  250.3 58.4 reduce-scatter.1
